TPU v7x, 256 devices: a 4x2x16 block of a 4x16x16 slice. The times are simulated.
256 devices in a mesh: grp: 2 (over y), sp: 16 (over z), tp: 8 (over x, core).
Axes of the slice: x: 4, y: 2, z: 16, core: 2. Of those that a mesh axis runs over, the one named last changes fastest.
The devices are a block of a 4x16x16 slice.
Arguments:
- tokens: bfloat16 [16384, 2, 2048], P(('grp', 'sp', 'tp')), parts along dimension 0, may hold values from -64 to 64
- w_query: bfloat16 [2048, 2048], P(None, 'tp'), may hold values from -0.21875 to 0.21875
- w_key: bfloat16 [2048, 2048], P(None, 'tp'), may hold values from -0.125 to 0.125
- w_value: bfloat16 [2048, 2048], P(None, 'tp'), may hold values from -0.125 to 0.125
- w_out: bfloat16 [2048, 2048], P('tp'), may hold values from -0.125 to 0.125
- head_lambda: float32 [16], P('tp'), may hold values from 0.3 to 0.8
- sub_gain: float32 [128], replicated, may hold values from 0.1 to 1.9
Outputs:
- mixed: bfloat16 [16384, 2, 2048], P(('grp', 'sp', 'tp')), parts along dimension 0
There are 2 independent parts, one for each index of `grp`. A program takes and returns all parts, laid end to end along the dimension named above; an argument that names none is the same for every part. Nothing has to cross between parts.
All inputs are finite; a program needn't handle non-finite values.
Results may differ from a plain program's by a relative error of at most 0.015.
The roundings to bfloat16 on the way count: a program that leaves them out, or rounds other values in their place, can miss the bound.
Values may be sent and summed in bfloat16 or wider, within the bound.
A program may use at most 128 MiB of HBM per device.

v0:
```python
import math

import jax
import jax.numpy as jnp
from jax import lax
from jax.sharding import PartitionSpec as P

SPAN = 64


NEG_FILL = -1e30
EPS_NORM = 1e-06


def sent_together(arrays, axis, dim, along):
    widths = [a.shape[along] for a in arrays]
    both = jnp.concatenate(arrays, axis=along)
    filled = lax.all_gather(both, axis, axis=dim, tiled=True)
    return tuple(jnp.split(filled, [sum(widths[:k]) for k in range(1, len(widths))], axis=along))


def cut_along(value, dim, length):
    shape = value.shape
    tiles = value.reshape(*shape[:dim], length, shape[dim] // length, *shape[dim + 1 :])
    return jnp.moveaxis(tiles, dim, 0)


def summed_on_arrival(value, axis, dim):
    tiles = cut_along(value, dim, lax.axis_size(axis))
    arrived = lax.all_to_all(tiles, axis, split_axis=0, concat_axis=0, tiled=True)
    return arrived.astype(jnp.float32).sum(axis=0)


def key_block(state_in, queries, query_pos, key_blk, value_blk, key_start):
    run_max, run_sum, run_acc = state_in
    blk_len = key_blk.shape[0]
    heads_here = queries.shape[1]
    head_dim = queries.shape[3]
    key_pos = key_start + jnp.arange(blk_len, dtype=jnp.int32)
    key_four = key_blk.reshape(blk_len, heads_here, 2, head_dim)
    scores = jnp.einsum("qhmd,khmd->mhqk", queries, key_four, preferred_element_type=jnp.float32)
    scores = scores * head_dim ** (-0.5)
    allowed = (key_pos // SPAN)[None, :] <= (query_pos // SPAN)[:, None]
    new_max = jnp.maximum(run_max, jnp.max(jnp.where(allowed, scores, NEG_FILL), axis=-1))
    expo_vals = jnp.where(allowed, jnp.exp(scores - new_max[..., None]), 0.0)
    factor = jnp.exp(run_max - new_max)
    run_sum = run_sum * factor + jnp.sum(expo_vals, axis=-1)
    value_three = value_blk.reshape(blk_len, heads_here, 2 * head_dim)
    mixed_vals = jnp.einsum(
        "mhqk,khe->mhqe",
        expo_vals.astype(jnp.bfloat16),
        value_three,
        preferred_element_type=jnp.float32,
    )
    run_acc = run_acc * factor[..., None] + mixed_vals
    return (new_max, run_sum, run_acc)


def guarded_block(state_in, queries, query_pos, key_blk, value_blk, key_start):
    last_pos = query_pos[-1]

    def compute(inner_state):
        return key_block(inner_state, queries, query_pos, key_blk, value_blk, key_start)

    def keep(inner_state):
        return inner_state

    return lax.cond(key_start <= last_pos, compute, keep, state_in)


def sequence_piece(state_in, queries, query_pos, key_part, value_part):
    length = key_part.shape[0]
    step_len = math.gcd(length, 512)
    step_count = length // step_len

    def one_step(step_index, inner_state):
        offset = step_index * step_len
        key_blk = lax.dynamic_slice_in_dim(key_part, offset, step_len, 0)
        value_blk = lax.dynamic_slice_in_dim(value_part, offset, step_len, 0)
        return guarded_block(inner_state, queries, query_pos, key_blk, value_blk, offset)

    return lax.fori_loop(0, step_count, one_step, state_in)


def normalize(attn, sub_gain):
    mean_sq = jnp.mean(attn * attn, axis=-1, keepdims=True)
    normed = (attn * lax.rsqrt(mean_sq + EPS_NORM) * sub_gain).astype(jnp.bfloat16)
    return jnp.transpose(normed, (1, 0, 2)).reshape(attn.shape[1], attn.shape[0] * attn.shape[2])


def on_device(tokens, w_query, w_key, w_value, w_out, head_lambda, sub_gain):
    tp_count = lax.axis_size("tp")
    tok_rows = tokens.shape[0] * tp_count
    seq_count = tokens.shape[1]
    heads_here = head_lambda.shape[0]
    head_dim = w_query.shape[1] // (2 * heads_here)
    value_dim = 2 * head_dim
    query_cols = w_query.shape[1]
    w_joined = jnp.concatenate([w_query, w_key, w_value], axis=1)
    joined = jnp.dot(
        lax.all_gather(tokens, "tp", axis=0, tiled=True),
        w_joined,
        preferred_element_type=jnp.float32,
    ).astype(jnp.bfloat16)
    query_flat = joined[:, :, :query_cols]
    keys_here = joined[:, :, query_cols : 2 * query_cols]
    values_here = joined[:, :, 2 * query_cols :]
    sp_index = lax.axis_index("sp")
    own_first = sp_index * tok_rows
    lam_col = head_lambda[:, None, None]

    def attend(query_sets, first_rows):
        positions = [first + jnp.arange(tok_rows, dtype=jnp.int32) for first in first_rows]
        query_four = [qset.reshape(tok_rows, heads_here, 2, head_dim) for qset in query_sets]
        start_one = (
            jnp.full((2, heads_here, tok_rows), NEG_FILL, jnp.float32),
            jnp.zeros((2, heads_here, tok_rows), jnp.float32),
            jnp.zeros((2, heads_here, tok_rows, value_dim), jnp.float32),
        )
        start_state = tuple((start_one for seq_index in range(seq_count)))
        key_part, value_part = sent_together((keys_here, values_here), "sp", 0, 1)
        new_states = []
        for seq_index in range(seq_count):
            new_states.append(
                sequence_piece(
                    start_state[seq_index],
                    query_four[seq_index],
                    positions[seq_index],
                    key_part[:, seq_index],
                    value_part[:, seq_index],
                )
            )
        final_states = tuple(new_states)
        results = []
        for run_max, run_sum, run_acc in final_states:
            attn = run_acc[0] / run_sum[0][..., None] - lam_col * run_acc[1] / run_sum[1][..., None]
            results.append(normalize(attn, sub_gain))
        return results

    normed_list = attend(
        [query_flat[:, seq_index] for seq_index in range(seq_count)],
        [own_first for seq_index in range(seq_count)],
    )
    normed = jnp.stack(normed_list, axis=1)
    summed = summed_on_arrival(
        jnp.dot(normed, w_out, preferred_element_type=jnp.float32).astype(jnp.bfloat16), "tp", 0
    )
    return summed.astype(jnp.bfloat16)


def solution(mesh):
    return jax.shard_map(
        on_device,
        mesh=mesh,
        in_specs=(
            P(("grp", "sp", "tp"), None, None),
            P(None, "tp"),
            P(None, "tp"),
            P(None, "tp"),
            P("tp", None),
            P("tp"),
            P(),
        ),
        out_specs=P(("grp", "sp", "tp"), None, None),
        check_vma=False,
    )
```

profile of v0, /device:TPU:1952, one launch (start us, length us, event | category | flops | bytes accessed | tf_op | source)
XLA Modules:
  0.0 506.2 jit_solution(3310146499048308824)
XLA Ops:
  6.6 2.1 copy.57
  8.8 2.3 copy.54
  11.1 1.4 copy.55
  12.6 1.4 copy.56
  14.0 28.6 %all-gather.3.cloned.1.call-done = bf16[512,2,2048]{2,0,1:T(8,128)(2,1)} async-done(((bf16[64,2,2048]{2,0,1:T(8,128)(2,1)}), bf16[512,2,2048]{2,0,1:T(8,128)(2,1)}) %all-gather.3.cloned.1.call-update) | async-done | bytes 4194320 | tf_op jit(solution)/shard_map/all_gather | solution.py:101
  42.6 6.6 %fusion.46 = bf16[512,2,768]{0,2,1:T(8,128)(2,1)S(1)} fusion(bf16[512,2,2048]{2,0,1:T(8,128)(2,1)} %all-gather.3.cloned.1.call-done, bf16[2048,256]{0,1:T(8,128)(2,1)} %copy.56, bf16[2048,256]{0,1:T(8,128)(2,1)} %copy.55, bf16[2048,256]{0,1:T(8,128)(2,1)} %copy.54), kind=kOutput, calls=%fused_computation.80 | convolution fusion | flops 3231449088 | bytes 8912896 | tf_op jit(solution)/shard_map/dot_general | solution.py:100
  50.5 185.9 %all-gather.5.cloned.1.call-done = bf16[8192,4,256]{0,2,1:T(8,128)(2,1)} async-done(((bf16[512,4,256]{0,2,1:T(8,128)(2,1)}), bf16[8192,4,256]{0,2,1:T(8,128)(2,1)}) %all-gather.5.cloned.1.call-update) | async-done | bytes 16777232 | tf_op jit(solution)/shard_map/all_gather | solution.py:18
  236.4 12.2 %slice_bitcast_fusion.2 = (bf16[8192,256]{0,1:T(8,128)(2,1)}, bf16[8192,256]{0,1:T(8,128)(2,1)}, bf16[8192,256]{0,1:T(8,128)(2,1)}, bf16[8192,256]{0,1:T(8,128)(2,1)}) fusion(bf16[8192,4,256]{0,2,1:T(8,128)(2,1)} %all-gather.5.cloned.1.call-done), kind=kLoop, calls=%fused_computation.70 | loop fusion | bytes 33554432 | tf_op jit(solution)/shard_map/squeeze | solution.py:130
  248.7 92.8 %while.34 = (s32[]{:T(128)}, f32[2,2,512]{2,1,0:T(2,128)S(1)}, f32[2,2,512]{2,1,0:T(2,128)S(1)}, f32[2,2,512,128]{3,2,0,1:T(8,128)S(1)}, s32[512]{0:T(512)S(1)},...) while((s32[]{:T(128)}, f32[2,2,512]{2,1,0:T(2,128)S(1)}, ...), condition=%wide.region_5.6_spmd, body=%wide.region_0.5_spmd.sunk | while | flops 411848192 | bytes 17451304 | solution.py:82
  249.8 4.7 conditional.4
  253.1 1.4 fusion.10
  255.7 4.7 conditional.4
  261.5 4.7 conditional.4
  267.3 4.7 conditional.4
  273.1 4.7 conditional.4
  276.4 1.4 fusion.10
  278.9 4.7 conditional.4
  284.7 4.7 conditional.4
  290.5 4.7 conditional.4
  296.3 4.7 conditional.4
  302.1 4.7 conditional.4
  307.9 4.7 conditional.4
  313.7 4.7 conditional.4
  319.5 4.7 conditional.4
  325.3 4.7 conditional.4
  331.1 4.7 conditional.4
  336.9 4.7 conditional.4
  341.7 95.1 %while.35 = (s32[]{:T(128)}, f32[2,2,512]{2,1,0:T(2,128)S(1)}, f32[2,2,512]{2,1,0:T(2,128)S(1)}, f32[2,2,512,128]{3,2,0,1:T(8,128)S(1)}, s32[512]{0:T(512)S(1)},...) while((s32[]{:T(128)}, f32[2,2,512]{2,1,0:T(2,128)S(1)}, ...), condition=%wide.region_12.13_spmd, body=%wide.region_7.12_spmd.sunk | while | flops 411848192 | bytes 17451304 | solution.py:82
  343.0 4.7 conditional.5
  348.9 4.7 conditional.5
  352.2 1.4 fusion.30
  354.9 4.7 conditional.5
  360.8 4.7 conditional.5
  366.8 4.7 conditional.5
  372.7 4.7 conditional.5
  378.7 4.7 conditional.5
  384.6 4.7 conditional.5
  390.5 4.7 conditional.5
  396.5 4.7 conditional.5
  402.4 4.7 conditional.5
  408.4 4.7 conditional.5
  414.3 4.7 conditional.5
  420.3 4.7 conditional.5
  426.2 4.7 conditional.5
  429.5 1.4 fusion.30
  432.2 4.7 conditional.5
  441.2 53.9 %all_to_all.5 = bf16[8,64,2,2048]{3,1,2,0:T(8,128)(2,1)} all-to-all(bf16[8,64,2,2048]{3,1,2,0:T(8,128)(2,1)S(1)} %copy.65), channel_id=1, replica_groups=mesh['grp'=2,'sp'=16,'tp'=8] {'tp'}, dimensions={0} | all-to-all | bytes 8388608 | tf_op jit(solution)/shard_map/all_to_all | solution.py:30
  495.1 2.9 reduce_sum.56
  (386 shorter events, 167.2 us)
Async XLA Ops:
  6.5 432.8 %copy-start = (bf16[256,2048]{1,0:T(8,128)(2,1)S(1)}, bf16[256,2048]{1,0:T(8,128)(2,1)}, u32[]{:S(2)}) copy-start(bf16[256,2048]{1,0:T(8,128)(2,1)} %param.19) | copy-start | bytes 3145732
  6.6 4.6 copy-start.1
  6.6 6.0 %copy-start.2 = (bf16[2048,256]{1,0:T(8,128)(2,1)S(1)}, bf16[2048,256]{1,0:T(8,128)(2,1)}, u32[]{:S(2)}) copy-start(bf16[2048,256]{1,0:T(8,128)(2,1)} %param.18) | copy-start | bytes 3145732
  6.6 36.0 %all-gather.3.cloned.1.call-start = ((), (), s32[]{:S(2)}) async-start(), calls=%async_computation.1 | async-start | bytes 4718592 | tf_op jit(solution)/shard_map/all_gather | solution.py:101
  8.8 227.7 %all-gather.5.cloned.1.call-start = ((), (), s32[]{:S(2)}) async-start(), calls=%async_computation.2 | async-start | bytes 17825792 | tf_op jit(solution)/shard_map/all_gather | solution.py:18
  341.7 95.2 %copy-start.4 = (f32[2]{0:T(128)S(1)}, f32[2]{0:T(128)}, u32[]{:S(2)}) copy-start(f32[2]{0:T(128)} %param.20) | copy-start | bytes 28
  341.7 96.4 %copy-start.3 = (f32[128]{0:T(128)S(1)}, f32[128]{0:T(128)}, u32[]{:S(2)}) copy-start(f32[128]{0:T(128)} %param.21) | copy-start | bytes 1540
Sparse Core Ops, SparseCore 0:
  9.2 33.3 all-gather.2
  50.5 185.8 all-gather.4
where the time goes:
time: 507 us; the launch traced here: 506 us
  waiting for transfers between devices  215 us (42%)
  matrix products  80.8 us (16%)
  local copies, waits for them, and re-layouts  75.7 us (15%)
  blocking collectives  53.9 us (11%)
  other arithmetic  44.9 us (9%)
  loops' own time  22.5 us (4%)
  between operations  13.7 us (3%)
    all_gather x1, waiting for transfers between devices, sent_together(): filled = lax.all_gather(both, axis, axis=dim, tiled=True)  186 us
    all_to_all x1, blocking collectives, summed_on_arrival(): lax.all_to_all(tiles, axis, split_axis=0, concat_axis=0, tiled=True)  53.9 us
    dot_general x32, matrix products, key_block(): jnp.einsum('mhqk,khe->mhqe', expo_vals.astype(jnp.bfloat16), value_three,...  43.9 us
    dynamic_slice x32, local copies, waits for them, and re-layouts, one_step(): value_blk = lax.dynamic_slice_in_dim(value_part, offset, step_len, 0)  34.4 us
    convert_element_type x32, other arithmetic, key_block(): expo_vals.astype(jnp.bfloat16)  31.2 us
    dot_general x32, matrix products, key_block(): jnp.einsum('qhmd,khmd->mhqk', queries, key_four, preferred_element_type=j...  29.1 us
    all_gather x1, waiting for transfers between devices, on_device(): lax.all_gather(tokens, 'tp', axis=0, tiled=True)  28.6 us
    another operation x2, loops' own time, sequence_piece(): return lax.fori_loop(0, step_count, one_step, state_in)  20 us
  transfers between devices with their start and end apart: 2, of which 2 were waited for; matrix products, arithmetic and copies ran while one was open for 1% of the time, Pallas kernels for 0%

commit v1 on v0

v1 whole, which is shorter than its diff:
```python
import functools

import jax
import jax.numpy as jnp
from jax import lax
from jax.experimental import pallas as pl
from jax.experimental.pallas import tpu as pltpu
from jax.sharding import PartitionSpec as P

SPAN = 64
NEG_FILL = -1e30
EPS_NORM = 1e-06
MESH = pl.DeviceIdType.MESH


def attend_kernel(
    n_sp,
    seqs,
    lam_ref,
    gain_ref,
    joined,
    out_ref,
    qbuf,
    kvbuf,
    ostage,
    lam_buf,
    qpad,
    top,
    acc,
    kv_sem,
    q_sem,
    o_sem,
    kv_send,
    q_send,
    o_send,
    fwd_core,
    fwd_chip,
    lam_sem,
):
    groups, _, rows, cols = joined.shape
    vdim = gain_ref.shape[1]
    head_dim = vdim // 2
    heads_here = cols // (3 * vdim)
    n_pairs = seqs * heads_here
    n_reg = n_sp // 2
    half = groups // 2
    chunk = half * rows
    tok_rows = groups * rows

    z = lax.axis_index("sp")
    tp = lax.axis_index("tp")
    core = lax.rem(tp, 2)
    chip_base = tp - core
    region = z // 2
    odd = lax.rem(z, 2)
    source_core = lax.rem(region, 2)
    pair = region // 2
    home_head, home_seq = pair // seqs, lax.rem(pair, seqs)
    rank = odd * 2 + core

    def dev(zz, cc):
        return {"sp": zz, "tp": chip_base + cc}

    def remote(src, dst, send, recv, zz, cc):
        return pltpu.make_async_remote_copy(
            src_ref=src, dst_ref=dst, send_sem=send, recv_sem=recv, device_id=dev(zz, cc), device_id_type=MESH
        )

    def entry_of(reg, zz):
        ahead = lax.rem(reg - zz // 2 + n_reg, n_reg)
        up = jnp.logical_or(ahead < n_reg // 2, jnp.logical_and(ahead == n_reg // 2, lax.rem(zz, 2) == 1))
        return jnp.where(ahead == 0, zz, jnp.where(up, 2 * reg, 2 * reg + 1))

    barrier = pltpu.get_barrier_semaphore()

    def greet(i, carry):
        zz, cc = i // 2, lax.rem(i, 2)

        @pl.when(jnp.logical_or(zz != z, cc != core))
        def _():
            pl.semaphore_signal(barrier, inc=1, device_id=dev(zz, cc), device_id_type=MESH)

        return carry

    lax.fori_loop(0, 2 * n_sp, greet, 0)
    pl.semaphore_wait(barrier, 2 * n_sp - 1)

    lam_copy = remote(lam_ref, lam_buf, lam_sem.at[0], lam_sem.at[1], z, 1 - core)
    lam_copy.start()

    def kv_src(k):
        head, seq = k // seqs, k % seqs
        return joined.at[:, seq, :, 2 * vdim * head : 2 * vdim * (head + 1)]

    for k in range(n_pairs):
        reg = 2 * k + core
        ent = entry_of(reg, z)
        here = ent == z

        @pl.when(here)
        def _():
            pltpu.make_async_copy(kv_src(k), kvbuf.at[z], kv_sem.at[z]).start()

        @pl.when(jnp.logical_not(here))
        def _():
            remote(kv_src(k), kvbuf.at[z], kv_send.at[k], kv_sem.at[z], ent, core).start()

    def q_src(k, b):
        head, seq = k // seqs, k % seqs
        first = (2 * heads_here + head) * vdim
        return joined.at[half * b : half * (b + 1), seq, :, first : first + vdim]

    def q_place(b):
        t = 2 * z + b
        u = lax.rem(t, 8)
        rk = jnp.where(u < 4, u, 7 - u)
        return rk // 2, lax.rem(rk, 2), (t // 8) * 2 + u // 4

    for b in range(2):
        rz, rc, slot = q_place(b)
        for k in range(n_pairs):
            zz = 2 * (2 * k + core) + rz
            here = jnp.logical_and(zz == z, rc == core)

            @pl.when(here)
            def _():
                pltpu.make_async_copy(q_src(k, b), qbuf.at[slot], q_sem.at[slot]).start()

            @pl.when(jnp.logical_not(here))
            def _():
                remote(q_src(k, b), qbuf.at[slot], q_send.at[2 * k + b], q_sem.at[slot], zz, rc).start()

    def arrive(n, carry):
        d = (n + 1) // 2
        zz = lax.rem(z + jnp.where(lax.rem(n, 2) == 1, d, n_sp - d), n_sp)
        pltpu.make_async_copy(kvbuf.at[zz], kvbuf.at[zz], kv_sem.at[zz]).wait()

        @pl.when(core == source_core)
        def _():
            @pl.when(entry_of(region, zz) == z)
            def _():
                remote(kvbuf.at[zz], kvbuf.at[zz], fwd_chip.at[zz], kv_sem.at[zz], z + 1 - 2 * odd, core).start()

            remote(kvbuf.at[zz], kvbuf.at[zz], fwd_core.at[zz], kv_sem.at[zz], z, 1 - core).start()

        return carry

    lax.fori_loop(0, n_sp, arrive, 0)
    lam_copy.wait()

    step_shards = 2
    step_keys = step_shards * tok_rows
    lam_rows = jnp.where(core == source_core, lam_ref[...], lam_buf[...])
    lam_row = lam_rows[0:1]
    for head in range(1, heads_here):
        lam_row = jnp.where(home_head == head, lam_rows[head : head + 1], lam_row)
    gain = gain_ref[...]
    lanes = lax.broadcasted_iota(jnp.int32, (chunk, vdim), 1)
    ones = jnp.ones((step_keys, vdim), jnp.bfloat16)

    def key_step(j, first_row):
        kv = kvbuf[pl.ds(j * step_shards, step_shards)].reshape(step_keys, 2 * vdim)
        keys = kv[:, :vdim]
        vals = jnp.concatenate([kv[:, vdim:], ones], axis=1)
        for m in range(2):
            here = slice(m * chunk, (m + 1) * chunk)
            scores = lax.dot_general(
                qpad[here], keys, (((1,), (1,)), ((), ())), preferred_element_type=jnp.float32
            )
            if first_row is not None:
                key_pos = j * step_keys + lax.broadcasted_iota(jnp.int32, (chunk, step_keys), 1)
                query_pos = first_row + lax.broadcasted_iota(jnp.int32, (chunk, step_keys), 0)
                scores = jnp.where(key_pos // SPAN <= query_pos // SPAN, scores, NEG_FILL)
            old = top[here]
            new = jnp.maximum(old, jnp.max(scores, axis=1, keepdims=True))
            expo = jnp.exp(scores - new[:, :1]).astype(jnp.bfloat16)
            factor = jnp.exp(old - new)
            acc[here] = acc[here] * jnp.concatenate([factor, factor], axis=1) + jnp.dot(
                expo, vals, preferred_element_type=jnp.float32
            )
            top[here] = new

    def o_dst(pr, b):
        head, seq = pr // seqs, lax.rem(pr, seqs)
        return out_ref.at[pl.ds(b * half, half), seq, :, pl.ds(pl.multiple_of(head * vdim, vdim), vdim)]

    def one_chunk(n, carry):
        t = (n // 2) * 8 + jnp.where(lax.rem(n, 2) == 1, 7 - rank, rank)
        pltpu.make_async_copy(qbuf.at[n], qbuf.at[n], q_sem.at[n]).wait()
        query = (qbuf[n].reshape(chunk, vdim).astype(jnp.float32) * head_dim ** (-0.5))
        qpad[:chunk] = jnp.where(lanes < head_dim, query, 0.0).astype(jnp.bfloat16)
        qpad[chunk:] = jnp.where(lanes < head_dim, 0.0, query).astype(jnp.bfloat16)
        top[...] = jnp.full(top.shape, NEG_FILL, jnp.float32)
        acc[...] = jnp.zeros(acc.shape, jnp.float32)
        full = (t * chunk) // step_keys

        def body(j, c):
            key_step(j, None)
            return c

        lax.fori_loop(0, full, body, 0)
        key_step(full, t * chunk)
        first, second = acc[:chunk], acc[chunk:]
        attn = first[:, :vdim] / first[:, vdim:] - lam_row * second[:, :vdim] / second[:, vdim:]
        mean_sq = jnp.mean(attn * attn, axis=1, keepdims=True)
        normed = attn * lax.rsqrt(mean_sq + EPS_NORM) * gain
        ostage[n] = normed.astype(jnp.bfloat16).reshape(half, rows, vdim)
        b, zz = lax.rem(t, 2), t // 2
        here = jnp.logical_and(zz == z, core == source_core)

        @pl.when(here)
        def _():
            pltpu.make_async_copy(ostage.at[n], o_dst(pair, b), o_sem.at[2 * pair + b]).start()

        @pl.when(jnp.logical_not(here))
        def _():
            remote(ostage.at[n], o_dst(pair, b), o_send.at[n], o_sem.at[2 * pair + b], zz, source_core).start()

        return carry

    lax.fori_loop(0, n_sp // 2, one_chunk, 0)

    for k in range(n_pairs):
        for b in range(2):
            pltpu.make_async_copy(o_dst(jnp.int32(k), b), o_dst(jnp.int32(k), b), o_sem.at[2 * k + b]).wait()

    for k in range(n_pairs):
        @pl.when(entry_of(2 * k + core, z) != z)
        def _():
            remote(kv_src(k), kvbuf.at[z], kv_send.at[k], kv_sem.at[z], z, core).wait_send()

        for b in range(2):
            rz, rc, slot = q_place(b)

            @pl.when(jnp.logical_or(2 * (2 * k + core) + rz != z, rc != core))
            def _():
                remote(q_src(k, b), qbuf.at[slot], q_send.at[2 * k + b], q_sem.at[slot], z, core).wait_send()

    def drain(n, carry):
        t = (n // 2) * 8 + jnp.where(lax.rem(n, 2) == 1, 7 - rank, rank)

        @pl.when(jnp.logical_or(t // 2 != z, core != source_core))
        def _():
            remote(ostage.at[n], ostage.at[n], o_send.at[n], q_sem.at[n], z, core).wait_send()

        return carry

    lax.fori_loop(0, n_sp // 2, drain, 0)

    @pl.when(core == source_core)
    def _():
        def sent(zz, carry):
            @pl.when(entry_of(region, zz) == z)
            def _():
                remote(kvbuf.at[zz], kvbuf.at[zz], fwd_chip.at[zz], kv_sem.at[zz], z, core).wait_send()

            remote(kvbuf.at[zz], kvbuf.at[zz], fwd_core.at[zz], kv_sem.at[zz], z, core).wait_send()
            return carry

        lax.fori_loop(0, n_sp, sent, 0)


def attend(joined, head_lambda, sub_gain, n_sp):
    groups, seqs, rows, cols = joined.shape
    heads_here = head_lambda.shape[0]
    vdim = sub_gain.shape[0]
    half = groups // 2
    chunk = half * rows
    n_pairs = seqs * heads_here
    n_chunks = n_sp // 2
    lam = jnp.broadcast_to(jnp.pad(head_lambda, (0, 8 - heads_here))[:, None], (8, vdim))
    dma = pltpu.SemaphoreType.DMA
    return pl.pallas_call(
        functools.partial(attend_kernel, n_sp, seqs),
        name="attend",
        out_shape=jax.ShapeDtypeStruct((groups, seqs, rows, heads_here * vdim), jnp.bfloat16),
        in_specs=[
            pl.BlockSpec(memory_space=pltpu.VMEM),
            pl.BlockSpec(memory_space=pltpu.VMEM),
            pl.BlockSpec(memory_space=pltpu.HBM),
        ],
        out_specs=pl.BlockSpec(memory_space=pltpu.HBM),
        scratch_shapes=[
            pltpu.VMEM((n_chunks, half, rows, vdim), jnp.bfloat16),
            pltpu.VMEM((n_sp, groups, rows, 2 * vdim), jnp.bfloat16),
            pltpu.VMEM((n_chunks, half, rows, vdim), jnp.bfloat16),
            pltpu.VMEM((8, vdim), jnp.float32),
            pltpu.VMEM((2 * chunk, vdim), jnp.bfloat16),
            pltpu.VMEM((2 * chunk, vdim), jnp.float32),
            pltpu.VMEM((2 * chunk, 2 * vdim), jnp.float32),
            dma((n_sp,)),
            dma((n_chunks,)),
            dma((2 * n_pairs,)),
            dma((n_pairs,)),
            dma((2 * n_pairs,)),
            dma((n_chunks,)),
            dma((n_sp,)),
            dma((n_sp,)),
            dma((2,)),
        ],
        compiler_params=pltpu.CompilerParams(
            collective_id=0, has_side_effects=True, vmem_limit_bytes=48 * 1024 * 1024
        ),
    )(lam, sub_gain[None, :], joined)


def on_device(n_sp, tokens, w_query, w_key, w_value, w_out, head_lambda, sub_gain):
    heads_here = head_lambda.shape[0]
    vdim = sub_gain.shape[0]
    parts = []
    for head in range(heads_here):
        cut = slice(head * vdim, (head + 1) * vdim)
        parts += [w_key[:, cut], w_value[:, cut]]
    w_joined = jnp.concatenate(parts + [w_query], axis=1)
    turned = jnp.transpose(tokens, (1, 0, 2))
    gathered = lax.all_gather(turned, "tp", axis=0, tiled=False)
    joined = jnp.dot(gathered, w_joined, preferred_element_type=jnp.float32).astype(jnp.bfloat16)
    normed = attend(joined, head_lambda, sub_gain, n_sp)
    partial = jnp.dot(normed, w_out, preferred_element_type=jnp.float32).astype(jnp.bfloat16)
    arrived = lax.all_to_all(partial, "tp", split_axis=0, concat_axis=0, tiled=True)
    summed = arrived.astype(jnp.float32).sum(axis=0).astype(jnp.bfloat16)
    return jnp.transpose(summed, (1, 0, 2))


def solution(mesh):
    return jax.shard_map(
        functools.partial(on_device, mesh.shape["sp"]),
        mesh=mesh,
        in_specs=(
            P(("grp", "sp", "tp"), None, None),
            P(None, "tp"),
            P(None, "tp"),
            P(None, "tp"),
            P("tp", None),
            P("tp"),
            P(),
        ),
        out_specs=P(("grp", "sp", "tp"), None, None),
        check_vma=False,
    )
```

time: 507 us -> 289 us (0.57)
  the two profiles are of different devices: /device:TPU:1952 before, /device:TPU:33 now
where the time goes in v1:
time: 289 us
  Pallas kernels  155 us (54%)
  blocking collectives  52.3 us (18%)
  waiting for transfers between devices  46.1 us (16%)
  between operations  13.5 us (5%)
  local copies, waits for them, and re-layouts  11.1 us (4%)
  matrix products  7.84 us (3%)
  other arithmetic  2.95 us (1%)
    pallas_call x1, Pallas kernels, attend(): pl.pallas_call(functools.partial(attend_kernel, n_sp, seqs), name='attend...  155 us
    all_to_all x1, blocking collectives, on_device(): lax.all_to_all(partial, 'tp', split_axis=0, concat_axis=0, tiled=True)  52.3 us
    all_gather x1, waiting for transfers between devices, on_device(): gathered = lax.all_gather(turned, 'tp', axis=0, tiled=False)  46.1 us
    unnamed x15, local copies, waits for them, and re-layouts  7.78 us
    dot_general x1, matrix products, on_device(): jnp.dot(gathered, w_joined, preferred_element_type=jnp.float32)  6.58 us
  transfers between devices with their start and end apart: 1, of which 1 were waited for; matrix products, arithmetic and copies ran while one was open for 3% of the time, Pallas kernels for 0%

profile of v1, /device:TPU:33, one launch (start us, length us, event | category | flops | bytes accessed | tf_op | source)
XLA Modules:
  0.0 288.9 jit_solution(17346251117991528498)
XLA Ops:
  6.5 0.0 copy-start
  6.6 0.0 copy-start.2
  6.6 0.0 copy-start.3
  6.6 0.0 all-gather.3.cloned.1.call-start
  6.6 2.1 copy.13
  8.7 0.1 all-gather.3.cloned.1.call-update
  8.8 0.0 copy-start.4
  8.8 0.7 pad.4
  9.5 1.9 slice_dynamic-update-slice_fusion.3
  11.5 1.9 slice_dynamic-update-slice_fusion.2
  13.4 0.0 copy-done.2
  13.4 0.9 slice_dynamic-update-slice_fusion.1
  14.3 0.0 copy-done.3
  14.3 0.9 slice_dynamic-update-slice_fusion
  15.2 0.0 copy-done.4
  15.2 1.1 constant_dynamic-update-slice_fusion
  16.3 46.1 %all-gather.3.cloned.1.call-done = bf16[16,64,2048]{2,1,0:T(8,128)(2,1)} async-done(((bf16[2,64,2048]{2,1,0:T(8,128)(2,1)}), bf16[16,64,2048]{2,1,0:T(8,128)(2,1)}) %all-gather.3.cloned.1.call-update) | async-done | bytes 4194320 | tf_op jit(solution)/shard_map/all_gather | solution.py:316
  62.4 0.0 copy-start.1
  62.4 6.6 %fusion.5.joined = bf16[8,2,64,768]{3,2,1,0:T(8,128)(2,1)S(1)} fusion(bf16[8,2,64,2048]{3,2,1,0:T(8,128)(2,1)} %bitcast.27, bf16[2048,768]{1,0:T(8,128)(2,1)} %constant_dynamic-update-slice_fusion), kind=kOutput, calls=%fused_computation.4 | convolution fusion | flops 3222011904 | bytes 8912896 | tf_op jit(solution)/shard_map/dot_general | solution.py:317
  69.0 0.1 broadcast_in_dim.4.lam_ref
  69.0 0.0 copy-done.1
  69.0 155.2 %attend.1 = bf16[8,2,64,256]{3,2,1,0:T(8,128)(2,1)S(1)} custom-call(f32[8,128]{1,0:T(8,128)S(1)} %broadcast_in_dim.4.lam_ref, f32[1,128]{1,0:T(1,128)S(1)} %bitcast.24, bf16[8,2,64,768]{3,2,1,0:T(8,128)(2,1)S(1)} %fusion.5.joined), custom_call_target="tpu_custom_call" | custom-call | tf_op jit(solution)/shard_map/attend/pallas_call | solution.py:273
  224.2 0.0 copy-done
  224.2 1.3 convolution_convert_fusion
  225.5 52.3 %all_to_all.5 = bf16[8,2,64,2048]{3,2,1,0:T(8,128)(2,1)} all-to-all(bf16[8,2,64,2048]{3,2,1,0:T(8,128)(2,1)S(1)} %convolution_convert_fusion), channel_id=1, replica_groups=mesh['grp'=2,'sp'=16,'tp'=8] {'tp'}, dimensions={0} | all-to-all | bytes 8388608 | tf_op jit(solution)/shard_map/all_to_all | solution.py:320
  277.8 2.9 %reduce_sum.12 = bf16[2,64,2048]{2,1,0:T(8,128)(2,1)S(1)} reduce(bf16[8,2,64,2048]{3,2,1,0:T(8,128)(2,1)} %all_to_all.5, bf16[]{:T(256)} %constant.5.clone.1), dimensions={0}, to_apply=%region_0.1 | reduce | flops 1835008 | bytes 4718594 | tf_op jit(solution)/shard_map/reduce_sum | solution.py:321
  280.8 1.3 copy.9
Async XLA Ops:
  6.5 217.7 %copy-start = (bf16[256,2048]{1,0:T(8,128)(2,1)S(1)}, bf16[256,2048]{1,0:T(8,128)(2,1)}, u32[]{:S(2)}) copy-start(bf16[256,2048]{1,0:T(8,128)(2,1)} %param.11) | copy-start | bytes 3145732
  6.6 6.9 %copy-start.2 = (bf16[2048,256]{1,0:T(8,128)(2,1)S(1)}, bf16[2048,256]{1,0:T(8,128)(2,1)}, u32[]{:S(2)}) copy-start(bf16[2048,256]{1,0:T(8,128)(2,1)} %param.9) | copy-start | bytes 3145732
  6.6 7.7 %copy-start.3 = (bf16[2048,256]{1,0:T(8,128)(2,1)S(1)}, bf16[2048,256]{1,0:T(8,128)(2,1)}, u32[]{:S(2)}) copy-start(bf16[2048,256]{1,0:T(8,128)(2,1)} %param.10) | copy-start | bytes 3145732
  6.6 55.8 %all-gather.3.cloned.1.call-start = ((), (), s32[]{:S(2)}) async-start(), calls=%async_computation.1 | async-start | bytes 4718592 | tf_op jit(solution)/shard_map/all_gather | solution.py:316
  8.8 6.4 %copy-start.4 = (bf16[2048,256]{1,0:T(8,128)(2,1)S(1)}, bf16[2048,256]{1,0:T(8,128)(2,1)}, u32[]{:S(2)}) copy-start(bf16[2048,256]{1,0:T(8,128)(2,1)} %param.8) | copy-start | bytes 3145732
  62.4 6.7 %copy-start.1 = (f32[128]{0:T(128)S(1)}, f32[128]{0:T(128)}, u32[]{:S(2)}) copy-start(f32[128]{0:T(128)} %param.13) | copy-start | bytes 1540
Sparse Core Ops, SparseCore 0:
  9.2 53.0 all-gather.2

commit v2 on v1

v2 whole, which is shorter than its diff:
```python
import functools

import jax
import jax.numpy as jnp
from jax import lax
from jax.experimental import pallas as pl
from jax.experimental.pallas import tpu as pltpu
from jax.sharding import PartitionSpec as P

SPAN = 64
NEG_FILL = -1e30
EPS_NORM = 1e-06
LEAD = 2
QUOTA = 5
MESH = pl.DeviceIdType.MESH


def layer_kernel(
    n_sp,
    turned,
    wq_ref,
    wk_ref,
    wv_ref,
    wo_ref,
    lam_ref,
    gain_ref,
    out_ref,
    tok,
    jbuf,
    qbuf,
    kvbuf,
    ostage,
    nbuf,
    lam_buf,
    qpad,
    top,
    acc,
    mine,
    sib_out,
    sib_in,
    xs,
    xr,
    ag_recv,
    ag_half,
    ag_send,
    kv_sem,
    q_sem,
    o_sem,
    kv_send,
    q_send,
    o_send,
    fwd_core,
    fwd_chip,
    lam_sem,
    sib_send,
    sib_recv,
    x_send,
    x_recv,
):
    seqs, groups, rows, _ = jbuf.shape
    width = tok.shape[3]
    vdim = gain_ref.shape[1]
    head_dim = vdim // 2
    heads_here = wq_ref.shape[1] // vdim
    n_pairs = seqs * heads_here
    n_reg = n_sp // 2
    n_x = groups // 2
    half = groups // 2
    chunk = half * rows
    tok_rows = groups * rows
    n_chunks = n_sp // 2

    z = lax.axis_index("sp")
    tp = lax.axis_index("tp")
    core = lax.rem(tp, 2)
    x = tp // 2
    region = z // 2
    odd = lax.rem(z, 2)
    source_core = lax.rem(region, 2)
    is_primary = core == source_core
    pair = region // 2
    home_head, home_seq = pair // seqs, lax.rem(pair, seqs)
    rank = odd * 2 + core

    def tp_of(ahead, cc):
        return 2 * lax.rem(x + ahead + n_x, n_x) + cc

    def to(src, dst, send, recv, zz, tt):
        return pltpu.make_async_remote_copy(
            src_ref=src,
            dst_ref=dst,
            send_sem=send,
            recv_sem=recv,
            device_id={"sp": zz, "tp": tt},
            device_id_type=MESH,
        )

    def remote(src, dst, send, recv, zz, cc):
        return to(src, dst, send, recv, zz, 2 * x + cc)

    def got(ref, sem):
        pltpu.make_async_copy(ref, ref, sem).wait()

    def entry_of(reg, zz):
        ahead = lax.rem(reg - zz // 2 + n_reg, n_reg)
        up = jnp.logical_or(ahead < n_reg // 2, jnp.logical_and(ahead == n_reg // 2, lax.rem(zz, 2) == 1))
        return jnp.where(ahead == 0, zz, jnp.where(up, 2 * reg, 2 * reg + 1))

    barrier = pltpu.get_barrier_semaphore()

    def greet(i, carry):
        zz, cc = i // 2, lax.rem(i, 2)

        @pl.when(jnp.logical_or(zz != z, cc != core))
        def _():
            pl.semaphore_signal(barrier, inc=1, device_id={"sp": zz, "tp": 2 * x + cc}, device_id_type=MESH)

        return carry

    for ahead in (1, -1):
        pl.semaphore_signal(barrier, inc=1, device_id={"sp": z, "tp": tp_of(ahead, core)}, device_id_type=MESH)
    lax.fori_loop(0, 2 * n_sp, greet, 0)
    pl.semaphore_wait(barrier, 2 * n_sp + 1)

    low, high = slice(0, rows // 2), slice(rows // 2, rows)

    def gather_copies(s):
        own, back, fore, far = tp, tp_of(-1, core), tp_of(1, core), tp_of(2, core)

        def send(i, src, dst, sem, tt):
            return to(src, dst, ag_send.at[8 * s + i], sem, z, tt)

        sib = 2 * x + 1 - core

        def full(i, t, tt):
            return send(i, tok.at[s, t], tok.at[s, t], ag_recv.at[groups * s + t], tt)

        return (
            lambda: send(0, turned.at[s], tok.at[s, own], ag_recv.at[groups * s + own], fore),
            lambda: send(1, turned.at[s], tok.at[s, own], ag_recv.at[groups * s + own], back),
            lambda: send(2, turned.at[s], tok.at[s, own], ag_recv.at[groups * s + own], sib),
            lambda: send(3, tok.at[s, back, low], tok.at[s, back, low], ag_half.at[2 * s], fore),
            lambda: send(4, tok.at[s, fore, high], tok.at[s, fore, high], ag_half.at[2 * s + 1], back),
            lambda: full(5, back, sib),
            lambda: full(6, fore, sib),
            lambda: full(7, far, sib),
        )

    def gather_start(s):
        pltpu.make_async_copy(turned.at[s], tok.at[s, tp], ag_recv.at[groups * s + tp]).start()
        for copy in gather_copies(s)[:3]:
            copy().start()

    def gather_near(s):
        copies = gather_copies(s)
        for i, ahead in enumerate((-1, 1)):
            t = tp_of(ahead, core)
            got(tok.at[s, t], ag_recv.at[groups * s + t])
            copies[3 + i]().start()
            copies[5 + i]().start()

    def gather_far(s):
        t = tp_of(2, core)
        got(tok.at[s, t, low], ag_half.at[2 * s])
        got(tok.at[s, t, high], ag_half.at[2 * s + 1])
        gather_copies(s)[7]().start()
        got(tok.at[s, tp], ag_recv.at[groups * s + tp])
        for ahead in (0, 1, -1, 2):
            t = tp_of(ahead, 1 - core)
            got(tok.at[s, t], ag_recv.at[groups * s + t])

    def project(s):
        def tile(i, carry):
            at = pl.ds(i * half, half)
            block = tok[s, at].reshape(chunk, width)
            for ref, first, step in ((wk_ref, 0, 2 * vdim), (wv_ref, vdim, 2 * vdim), (wq_ref, n_pairs * vdim, vdim)):
                done = jnp.dot(block, ref[...], preferred_element_type=jnp.float32).astype(jnp.bfloat16)
                for head in range(heads_here):
                    jbuf[s, at, :, first + head * step : first + head * step + vdim] = done[
                        :, head * vdim : (head + 1) * vdim
                    ].reshape(half, rows, vdim)
            return carry

        lax.fori_loop(0, 2, tile, 0)

    def kv_src(k):
        head, seq = k // seqs, k % seqs
        return jbuf.at[seq, :, :, 2 * vdim * head : 2 * vdim * (head + 1)]

    def q_src(k, b):
        head, seq = k // seqs, k % seqs
        first = (2 * heads_here + head) * vdim
        return jbuf.at[seq, half * b : half * (b + 1), :, first : first + vdim]

    def q_place(b):
        t = 2 * z + b
        u = lax.rem(t, 8)
        rk = jnp.where(u < 4, u, 7 - u)
        return rk // 2, lax.rem(rk, 2), (t // 8) * 2 + u // 4

    def q_copy(k, b):
        rz, rc, slot = q_place(b)
        zz = 2 * (2 * k + core) + rz
        here = jnp.logical_and(zz == z, rc == core)
        return here, slot, lambda: remote(q_src(k, b), qbuf.at[slot], q_send.at[2 * k + b], q_sem.at[slot], zz, rc)

    def kv_copy(k):
        ent = entry_of(2 * k + core, z)
        return ent == z, lambda: remote(kv_src(k), kvbuf.at[z], kv_send.at[k], kv_sem.at[z], ent, core)

    def send_queries(s):
        for k in range(s, n_pairs, seqs):
            for b in range(2):
                here, slot, copy = q_copy(k, b)

                @pl.when(here)
                def _():
                    qbuf[slot] = q_src(k, b)[...]

                @pl.when(jnp.logical_not(here))
                def _():
                    copy().start()

    def send_keys():
        for k in range(n_pairs):
            here, _ = kv_copy(k)

            @pl.when(here)
            def _():
                remote(kv_src(k), kvbuf.at[z], fwd_chip.at[z], kv_sem.at[z], z + 1 - 2 * odd, core).start()
                remote(kv_src(k), kvbuf.at[z], fwd_core.at[z], kv_sem.at[z], z, 1 - core).start()
                kvbuf[z] = kv_src(k)[...]

        for near in (True, False):
            for k in range(n_pairs):
                here, copy = kv_copy(k)
                ahead = lax.rem(2 * k + core - region + n_reg, n_reg)
                close = jnp.minimum(ahead, n_reg - ahead) <= n_reg // 4

                @pl.when(jnp.logical_and(jnp.logical_not(here), close if near else jnp.logical_not(close)))
                def _():
                    copy().start()

    lam_copy = remote(lam_ref, lam_buf, lam_sem.at[0], lam_sem.at[1], z, 1 - core)
    lam_copy.start()
    gather_start(0)
    gather_near(0)
    gather_start(1)
    gather_far(0)
    project(0)
    send_queries(0)
    gather_near(1)
    gather_far(1)
    project(1)
    send_queries(1)
    send_keys()
    lam_copy.wait()

    lanes = lax.broadcasted_iota(jnp.int32, (chunk, vdim), 1)
    step_keys = 2 * tok_rows
    ones = jnp.ones((step_keys, vdim), jnp.bfloat16)

    def chunk_of(n):
        return (n // 2) * 8 + jnp.where(lax.rem(n, 2) == 1, 7 - rank, rank)

    def local_chunk(n):
        t = chunk_of(n)
        return jnp.logical_and(t // 2 == z, is_primary)

    def ready(n, carry):
        @pl.when(jnp.logical_not(local_chunk(n)))
        def _():
            got(qbuf.at[n], q_sem.at[n])

        query = qbuf[n].reshape(chunk, vdim).astype(jnp.float32) * head_dim ** (-0.5)
        qpad[n, :chunk] = jnp.where(lanes < head_dim, query, 0.0).astype(jnp.bfloat16)
        qpad[n, chunk:] = jnp.where(lanes < head_dim, 0.0, query).astype(jnp.bfloat16)
        top[n] = jnp.full(top.shape[1:], NEG_FILL, jnp.float32)
        acc[n] = jnp.zeros(acc.shape[1:], jnp.float32)
        return carry

    def block(n, reg, first_row):
        kv = kvbuf[pl.ds(2 * reg, 2)].reshape(step_keys, 2 * vdim)
        keys = kv[:, :vdim]
        vals = jnp.concatenate([kv[:, vdim:], ones], axis=1)
        for m in range(2):
            here = slice(m * chunk, (m + 1) * chunk)
            scores = lax.dot_general(
                qpad[n, here], keys, (((1,), (1,)), ((), ())), preferred_element_type=jnp.float32
            )
            if first_row is not None:
                row = first_row + lax.broadcasted_iota(jnp.int32, (chunk, 1), 0)
                limit = (row // SPAN + 1) * SPAN
                key = lax.broadcasted_iota(jnp.int32, (chunk, step_keys), 1)
                scores = jnp.where(key < limit, scores, NEG_FILL)
            old = top[n, here]
            new = jnp.maximum(old, jnp.max(scores, axis=1, keepdims=True))
            expo = jnp.exp(scores - new[:, :1]).astype(jnp.bfloat16)
            factor = jnp.exp(old - new)
            acc[n, here] = acc[n, here] * jnp.concatenate([factor, factor], axis=1) + jnp.dot(
                expo, vals, preferred_element_type=jnp.float32
            )
            top[n, here] = new

    def own_shard(zz):
        return jnp.logical_and(zz == z, is_primary)

    def side(direct, lap):
        above = (odd == 1) if direct else (odd == 0)
        return lax.rem(region + jnp.where(above, lap, n_reg - lap), n_reg), above

    def shard_at(direct, k):
        lap, second = (k + 1) // 2, lax.rem(k + 1, 2)
        reg, above = side(direct, lap)
        far = jnp.where(k == n_reg - 1, 0, second)
        own = 2 * region + (odd if direct else 1 - odd)
        return jnp.where(k == 0, own, 2 * reg + jnp.where(above, far, 1 - far))

    def region_at(i):
        lap = (i + 1) // 2
        return jnp.where(lax.rem(i, 2) == 1, side(True, lap)[0], side(False, lap)[0])

    def use(p, c):
        reg, n = region_at(p // n_chunks), lax.rem(p, n_chunks)

        @pl.when(n > reg)
        def _():
            block(n, reg, None)

        @pl.when(n == reg)
        def _():
            block(n, reg, lax.rem(chunk_of(n), 4) * chunk)

        return c

    def take(zz, direct):
        @pl.when(jnp.logical_not(own_shard(zz)))
        def _():
            got(kvbuf.at[zz], kv_sem.at[zz])

            @pl.when(is_primary)
            def _():
                if direct:
                    remote(
                        kvbuf.at[zz], kvbuf.at[zz], fwd_chip.at[zz], kv_sem.at[zz], z + 1 - 2 * odd, core
                    ).start()
                remote(kvbuf.at[zz], kvbuf.at[zz], fwd_core.at[zz], kv_sem.at[zz], z, 1 - core).start()

    def arrive(i, used):
        @pl.when(i < n_reg)
        def _():
            take(shard_at(True, i), True)

        @pl.when(i == LEAD)
        def _():
            lax.fori_loop(0, n_chunks, ready, 0)

        def spend(used, done):
            whole = jnp.where(done < 1, 0, jnp.where(done == n_reg, n_reg, 2 * ((done - 1) // 2) + 2))
            whole = jnp.where(done == n_reg - 1, n_reg - 1, whole)
            upto = jnp.maximum(jnp.minimum(whole * n_chunks, used + QUOTA), used)
            lax.fori_loop(used, upto, use, 0)
            return upto

        used = spend(used, i - LEAD)

        @pl.when(i >= LEAD)
        def _():
            take(shard_at(False, i - LEAD), False)

        return spend(used, i - LEAD + 1)

    used = lax.fori_loop(0, n_reg + LEAD, arrive, jnp.int32(0))
    lax.fori_loop(used, n_reg * n_chunks, use, 0)

    lam_rows = jnp.where(is_primary, lam_ref[...], lam_buf[...])
    lam_row = lam_rows[0:1]
    for head in range(1, heads_here):
        lam_row = jnp.where(home_head == head, lam_rows[head : head + 1], lam_row)
    gain = gain_ref[...]

    def o_dst(pr, b):
        head, seq = pr // seqs, lax.rem(pr, seqs)
        return nbuf.at[pl.ds(b * n_x // 2, n_x // 2), :, seq, :, pl.ds(pl.multiple_of(head * vdim, vdim), vdim)]

    def finish(n, carry):
        t = chunk_of(n)
        first, second = acc[n, :chunk], acc[n, chunk:]
        attn = first[:, :vdim] / first[:, vdim:] - lam_row * second[:, :vdim] / second[:, vdim:]
        mean_sq = jnp.mean(attn * attn, axis=1, keepdims=True)
        normed = (attn * lax.rsqrt(mean_sq + EPS_NORM) * gain).astype(jnp.bfloat16).reshape(n_x // 2, 2, rows, vdim)
        b, zz = lax.rem(t, 2), t // 2
        here = local_chunk(n)
        ostage[n] = normed

        @pl.when(here)
        def _():
            o_dst(pair, b)[...] = normed

        @pl.when(jnp.logical_not(here))
        def _():
            remote(ostage.at[n], o_dst(pair, b), o_send.at[n], o_sem.at[2 * pair + b], zz, source_core).start()

        return carry

    lax.fori_loop(0, n_chunks, finish, 0)

    def partial(cc, s):
        block = nbuf[:, cc, s].reshape(n_x * rows, heads_here * vdim)
        done = jnp.dot(block, wo_ref[...], preferred_element_type=jnp.float32)
        return done.astype(jnp.bfloat16).reshape(n_x, rows, width)

    def sib_copy(s):
        return remote(sib_out.at[s], sib_in.at[s], sib_send.at[s], sib_recv.at[s], z, 1 - core)

    def both(s, ahead, part):
        to_x = lax.rem(x + ahead + n_x, n_x)
        return mine[s, to_x, part].astype(jnp.float32) + sib_in[s, to_x, part].astype(jnp.float32)

    ways = (1, -1, 1, -1, 1, -1)

    def x_copy(s, i):
        at = len(ways) * s + i
        return to(xs.at[at], xr.at[at], x_send.at[at], x_recv.at[at], z, tp_of(ways[i], core))

    def ship(s, i, value):
        xs[len(ways) * s + i] = value.astype(jnp.bfloat16)
        x_copy(s, i).start()

    def came(s, i):
        at = len(ways) * s + i
        got(xr.at[at], x_recv.at[at])
        return xr[at].astype(jnp.float32)

    def sum_start(s):
        for k in range(s, n_pairs, seqs):
            for b in range(2):
                here, _, _ = q_copy(k, b)

                @pl.when(jnp.logical_not(here))
                def _():
                    got(o_dst(jnp.int32(k), b), o_sem.at[2 * k + b])

        sib_out[s] = partial(1 - core, s)
        sib_copy(s).start()
        mine[s] = partial(core, s)
        got(sib_in.at[s], sib_recv.at[s])
        ship(s, 0, both(s, 2, low))
        ship(s, 1, both(s, 2, high))
        ship(s, 2, both(s, 1, high))
        ship(s, 3, both(s, -1, low))

    def sum_pass(s):
        ship(s, 4, both(s, 1, low) + came(s, 0))
        ship(s, 5, both(s, -1, high) + came(s, 1))

    def sum_end(s):
        out_ref[s, low] = (both(s, 0, low) + came(s, 3) + came(s, 4)).astype(jnp.bfloat16)
        out_ref[s, high] = (both(s, 0, high) + came(s, 2) + came(s, 5)).astype(jnp.bfloat16)

    sum_start(0)
    sum_pass(0)
    sum_start(1)
    sum_end(0)
    sum_pass(1)
    sum_end(1)

    for s in range(seqs):
        sib_copy(s).wait_send()
        for i in range(len(ways)):
            x_copy(s, i).wait_send()
    for s in range(seqs):
        for copy in gather_copies(s):
            copy().wait_send()
    for k in range(n_pairs):
        here, copy = kv_copy(k)

        @pl.when(jnp.logical_not(here))
        def _():
            copy().wait_send()

        for b in range(2):
            q_here, _, q_sent = q_copy(k, b)

            @pl.when(jnp.logical_not(q_here))
            def _():
                q_sent().wait_send()

    def drain(n, carry):
        @pl.when(jnp.logical_not(local_chunk(n)))
        def _():
            remote(ostage.at[n], ostage.at[n], o_send.at[n], q_sem.at[n], z, 1 - core).wait_send()

        return carry

    lax.fori_loop(0, n_chunks, drain, 0)

    @pl.when(is_primary)
    def _():
        def sent(zz, carry):
            @pl.when(entry_of(region, zz) == z)
            def _():
                remote(kvbuf.at[zz], kvbuf.at[zz], fwd_chip.at[zz], kv_sem.at[zz], z, 1 - core).wait_send()

            remote(kvbuf.at[zz], kvbuf.at[zz], fwd_core.at[zz], kv_sem.at[zz], z, 1 - core).wait_send()
            return carry

        lax.fori_loop(0, n_sp, sent, 0)


def on_device(n_sp, n_tp, tokens, w_query, w_key, w_value, w_out, head_lambda, sub_gain):
    rows, seqs, width = tokens.shape
    heads_here = head_lambda.shape[0]
    vdim = sub_gain.shape[0]
    half = n_tp // 2
    chunk = half * rows
    n_pairs = seqs * heads_here
    n_chunks = n_sp // 2
    lam = jnp.broadcast_to(jnp.pad(head_lambda, (0, 8 - heads_here))[:, None], (8, vdim))
    turned = jnp.transpose(tokens, (1, 0, 2))
    dma = pltpu.SemaphoreType.DMA
    bf16, f32 = jnp.bfloat16, jnp.float32
    in_vmem = pl.BlockSpec(memory_space=pltpu.VMEM)
    out = pl.pallas_call(
        functools.partial(layer_kernel, n_sp),
        name="layer",
        out_shape=jax.ShapeDtypeStruct((seqs, rows, width), bf16),
        in_specs=[pl.BlockSpec(memory_space=pltpu.HBM)] + [in_vmem] * 6,
        out_specs=in_vmem,
        scratch_shapes=[
            pltpu.VMEM((seqs, n_tp, rows, width), bf16),
            pltpu.VMEM((seqs, n_tp, rows, 3 * heads_here * vdim), bf16),
            pltpu.VMEM((n_chunks, half, rows, vdim), bf16),
            pltpu.VMEM((n_sp, n_tp, rows, 2 * vdim), bf16),
            pltpu.VMEM((n_chunks, n_tp // 4, 2, rows, vdim), bf16),
            pltpu.VMEM((n_tp // 2, 2, seqs, rows, heads_here * vdim), bf16),
            pltpu.VMEM((8, vdim), f32),
            pltpu.VMEM((n_chunks, 2 * chunk, vdim), bf16),
            pltpu.VMEM((n_chunks, 2 * chunk, vdim), f32),
            pltpu.VMEM((n_chunks, 2 * chunk, 2 * vdim), f32),
            pltpu.VMEM((seqs, n_tp // 2, rows, width), bf16),
            pltpu.VMEM((seqs, n_tp // 2, rows, width), bf16),
            pltpu.VMEM((seqs, n_tp // 2, rows, width), bf16),
            pltpu.VMEM((6 * seqs, rows // 2, width), bf16),
            pltpu.VMEM((6 * seqs, rows // 2, width), bf16),
            dma((seqs * n_tp,)),
            dma((2 * seqs,)),
            dma((8 * seqs,)),
            dma((n_sp,)),
            dma((n_chunks,)),
            dma((2 * n_pairs,)),
            dma((n_pairs,)),
            dma((2 * n_pairs,)),
            dma((n_chunks,)),
            dma((n_sp,)),
            dma((n_sp,)),
            dma((2,)),
            dma((seqs,)),
            dma((seqs,)),
            dma((6 * seqs,)),
            dma((6 * seqs,)),
        ],
        compiler_params=pltpu.CompilerParams(
            collective_id=0, has_side_effects=True, vmem_limit_bytes=60 * 1024 * 1024
        ),
    )(turned, w_query, w_key, w_value, w_out, lam, sub_gain[None, :])
    return jnp.transpose(out, (1, 0, 2))


def solution(mesh):
    return jax.shard_map(
        functools.partial(on_device, mesh.shape["sp"], mesh.shape["tp"]),
        mesh=mesh,
        in_specs=(
            P(("grp", "sp", "tp"), None, None),
            P(None, "tp"),
            P(None, "tp"),
            P(None, "tp"),
            P("tp", None),
            P("tp"),
            P(),
        ),
        out_specs=P(("grp", "sp", "tp"), None, None),
        check_vma=False,
    )
```

time: 289 us -> 209 us (0.72)
  the two profiles are of different devices: /device:TPU:33 before, /device:TPU:288 now
where the time goes in v2:
time: 209 us
  Pallas kernels  203 us (97%)
  local copies, waits for them, and re-layouts  5.68 us (3%)
    pallas_call x1, Pallas kernels, on_device(): pl.pallas_call(functools.partial(layer_kernel, n_sp), name='layer', out_s...  203 us

profile of v2, /device:TPU:288, one launch (start us, length us, event | category | flops | bytes accessed | tf_op | source)
XLA Modules:
  0.0 208.6 jit_solution(15394987634768460610)
XLA Ops:
  0.0 0.0 copy-start
  0.0 0.7 copy-done
  0.7 0.7 broadcast_in_dim.4.lam_ref
  1.3 2.0 copy.11
  3.3 202.9 %layer.1 = bf16[2,64,2048]{2,1,0:T(8,128)(2,1)} custom-call(bf16[2,64,2048]{2,1,0:T(8,128)(2,1)} %bitcast.6, bf16[2048,256]{1,0:T(8,128)(2,1)} %wq_ref.1, bf16[2048,256]{1,0:T(8,128)(2,1)} %wk_ref.1, bf16[2048,256]{1,0:T(8,128)(2,1)} %wv_ref.1, bf16[256,2048]{1,0:T(8,128)(2,1)} %wo_ref.1, f32[8,128]{1,0:T(8,128)} %broadcast_in_dim.4.lam_ref, f32[1,128]{1,0:T(1,128)} %bitcast.7), custom_call_target="tpu_custom_call" | custom-call | tf_op jit(solution)/shard_map/layer/pallas_call | solution.py:524
  206.3 2.4 %copy.9 = bf16[64,2,2048]{2,1,0:T(2,128)(2,1)} copy(bf16[64,2,2048]{2,0,1:T(8,128)(2,1)} %bitcast.5) | data formatting | bytes 1048576 | tf_op jit(solution)/shard_map/transpose | solution.py:567
  (1 shorter events, 0.0 us)
Async XLA Ops:
  0.0 0.7 copy-start

commit v3 on v2

--- a/solution.py
+++ b/solution.py
@@ -11,7 +11,7 @@
 NEG_FILL = -1e30
 EPS_NORM = 1e-06
 LEAD = 2
-QUOTA = 5
+QUOTA = 2
 MESH = pl.DeviceIdType.MESH
 
 
@@ -26,7 +26,8 @@
     gain_ref,
     out_ref,
     tok,
-    jbuf,
+    qj,
+    kvj,
     qbuf,
     kvbuf,
     ostage,
@@ -57,8 +58,7 @@
     x_send,
     x_recv,
 ):
-    seqs, groups, rows, _ = jbuf.shape
-    width = tok.shape[3]
+    seqs, groups, rows, width = tok.shape
     vdim = gain_ref.shape[1]
     head_dim = vdim // 2
     heads_here = wq_ref.shape[1] // vdim
@@ -171,26 +171,27 @@
 
     def project(s):
         def tile(i, carry):
-            at = pl.ds(i * half, half)
-            block = tok[s, at].reshape(chunk, width)
-            for ref, first, step in ((wk_ref, 0, 2 * vdim), (wv_ref, vdim, 2 * vdim), (wq_ref, n_pairs * vdim, vdim)):
-                done = jnp.dot(block, ref[...], preferred_element_type=jnp.float32).astype(jnp.bfloat16)
-                for head in range(heads_here):
-                    jbuf[s, at, :, first + head * step : first + head * step + vdim] = done[
-                        :, head * vdim : (head + 1) * vdim
-                    ].reshape(half, rows, vdim)
+            block = tok[s, pl.ds(i * half, half)].reshape(chunk, width)
+            at = pl.ds(pl.multiple_of(i * chunk, chunk), chunk)
+            keys = jnp.dot(block, wk_ref[...], preferred_element_type=jnp.float32).astype(jnp.bfloat16)
+            vals = jnp.dot(block, wv_ref[...], preferred_element_type=jnp.float32).T.astype(jnp.bfloat16)
+            queries = jnp.dot(block, wq_ref[...], preferred_element_type=jnp.float32).astype(jnp.bfloat16)
+            for head in range(heads_here):
+                k, cut = head * seqs + s, slice(head * vdim, (head + 1) * vdim)
+                qj[k, at] = queries[:, cut]
+                kvj[k, 0, at] = keys[:, cut]
+                for part in range(chunk // vdim):
+                    first = pl.multiple_of(i * chunk + part * vdim, vdim)
+                    kvj[k, 1, pl.ds(first, vdim)] = vals[cut, part * vdim : (part + 1) * vdim]
             return carry
 
         lax.fori_loop(0, 2, tile, 0)
 
     def kv_src(k):
-        head, seq = k // seqs, k % seqs
-        return jbuf.at[seq, :, :, 2 * vdim * head : 2 * vdim * (head + 1)]
+        return kvj.at[k]
 
     def q_src(k, b):
-        head, seq = k // seqs, k % seqs
-        first = (2 * heads_here + head) * vdim
-        return jbuf.at[seq, half * b : half * (b + 1), :, first : first + vdim]
+        return qj.at[k, b * chunk : (b + 1) * chunk]
 
     def q_place(b):
         t = 2 * z + b
@@ -256,9 +257,8 @@
     send_keys()
     lam_copy.wait()
 
-    lanes = lax.broadcasted_iota(jnp.int32, (chunk, vdim), 1)
-    step_keys = 2 * tok_rows
-    ones = jnp.ones((step_keys, vdim), jnp.bfloat16)
+    channel = lax.broadcasted_iota(jnp.int32, (vdim, chunk), 0)
+    ones = jnp.ones((acc.shape[1] - vdim, tok_rows), jnp.bfloat16)
 
     def chunk_of(n):
         return (n // 2) * 8 + jnp.where(lax.rem(n, 2) == 1, 7 - rank, rank)
@@ -272,35 +272,28 @@
         def _():
             got(qbuf.at[n], q_sem.at[n])
 
-        query = qbuf[n].reshape(chunk, vdim).astype(jnp.float32) * head_dim ** (-0.5)
-        qpad[n, :chunk] = jnp.where(lanes < head_dim, query, 0.0).astype(jnp.bfloat16)
-        qpad[n, chunk:] = jnp.where(lanes < head_dim, 0.0, query).astype(jnp.bfloat16)
+        query = qbuf[n].astype(jnp.float32).T * head_dim ** (-0.5)
+        qpad[n, :, :chunk] = jnp.where(channel < head_dim, query, 0.0).astype(jnp.bfloat16)
+        qpad[n, :, chunk:] = jnp.where(channel < head_dim, 0.0, query).astype(jnp.bfloat16)
         top[n] = jnp.full(top.shape[1:], NEG_FILL, jnp.float32)
         acc[n] = jnp.zeros(acc.shape[1:], jnp.float32)
         return carry
 
-    def block(n, reg, first_row):
-        kv = kvbuf[pl.ds(2 * reg, 2)].reshape(step_keys, 2 * vdim)
-        keys = kv[:, :vdim]
-        vals = jnp.concatenate([kv[:, vdim:], ones], axis=1)
-        for m in range(2):
-            here = slice(m * chunk, (m + 1) * chunk)
-            scores = lax.dot_general(
-                qpad[n, here], keys, (((1,), (1,)), ((), ())), preferred_element_type=jnp.float32
-            )
-            if first_row is not None:
-                row = first_row + lax.broadcasted_iota(jnp.int32, (chunk, 1), 0)
-                limit = (row // SPAN + 1) * SPAN
-                key = lax.broadcasted_iota(jnp.int32, (chunk, step_keys), 1)
-                scores = jnp.where(key < limit, scores, NEG_FILL)
-            old = top[n, here]
-            new = jnp.maximum(old, jnp.max(scores, axis=1, keepdims=True))
-            expo = jnp.exp(scores - new[:, :1]).astype(jnp.bfloat16)
-            factor = jnp.exp(old - new)
-            acc[n, here] = acc[n, here] * jnp.concatenate([factor, factor], axis=1) + jnp.dot(
-                expo, vals, preferred_element_type=jnp.float32
-            )
-            top[n, here] = new
+    def block(n, zz, first_row):
+        turned_vals = kvbuf[zz, 1].reshape(tok_rows // vdim, vdim, vdim)
+        vals = jnp.concatenate([turned_vals[i] for i in range(tok_rows // vdim)], axis=1)
+        vals = jnp.concatenate([vals, ones], axis=0)
+        scores = jnp.dot(kvbuf[zz, 0], qpad[n], preferred_element_type=jnp.float32)
+        if first_row is not None:
+            column = lax.broadcasted_iota(jnp.int32, (1, 2 * chunk), 1)
+            limit = ((first_row + lax.rem(column, chunk)) // SPAN + 1) * SPAN
+            key = lax.broadcasted_iota(jnp.int32, (tok_rows, 2 * chunk), 0)
+            scores = jnp.where(key < limit, scores, NEG_FILL)
+        old = top[n, 0:1]
+        new = jnp.maximum(old, jnp.max(scores, axis=0, keepdims=True))
+        expo = jnp.exp(scores - new).astype(jnp.bfloat16)
+        acc[n] = acc[n] * jnp.exp(old - new) + jnp.dot(vals, expo, preferred_element_type=jnp.float32)
+        top[n, 0:1] = new
 
     def own_shard(zz):
         return jnp.logical_and(zz == z, is_primary)
@@ -325,11 +318,18 @@
 
         @pl.when(n > reg)
         def _():
-            block(n, reg, None)
+            block(n, 2 * reg, None)
+            block(n, 2 * reg + 1, None)
 
         @pl.when(n == reg)
         def _():
-            block(n, reg, lax.rem(chunk_of(n), 4) * chunk)
+            last = lax.rem(chunk_of(n) // 2, 2)
+
+            @pl.when(last == 1)
+            def _():
+                block(n, 2 * reg, None)
+
+            block(n, 2 * reg + last, lax.rem(chunk_of(n), 2) * chunk)
 
         return c
 
@@ -371,7 +371,6 @@
         return spend(used, i - LEAD + 1)
 
     used = lax.fori_loop(0, n_reg + LEAD, arrive, jnp.int32(0))
-    lax.fori_loop(used, n_reg * n_chunks, use, 0)
 
     lam_rows = jnp.where(is_primary, lam_ref[...], lam_buf[...])
     lam_row = lam_rows[0:1]
@@ -385,10 +384,11 @@
 
     def finish(n, carry):
         t = chunk_of(n)
-        first, second = acc[n, :chunk], acc[n, chunk:]
-        attn = first[:, :vdim] / first[:, vdim:] - lam_row * second[:, :vdim] / second[:, vdim:]
-        mean_sq = jnp.mean(attn * attn, axis=1, keepdims=True)
-        normed = (attn * lax.rsqrt(mean_sq + EPS_NORM) * gain).astype(jnp.bfloat16).reshape(n_x // 2, 2, rows, vdim)
+        first, second = acc[n, :, :chunk], acc[n, :, chunk:]
+        attn = first[:vdim] / first[vdim : vdim + 1] - lam_row[:, :1] * second[:vdim] / second[vdim : vdim + 1]
+        mean_sq = jnp.mean(attn * attn, axis=0, keepdims=True)
+        normed = ((attn * lax.rsqrt(mean_sq + EPS_NORM)).T * gain).astype(jnp.bfloat16)
+        normed = normed.reshape(n_x // 2, 2, rows, vdim)
         b, zz = lax.rem(t, 2), t // 2
         here = local_chunk(n)
         ostage[n] = normed
@@ -403,7 +403,18 @@
 
         return carry
 
-    lax.fori_loop(0, n_chunks, finish, 0)
+    def rest(n, carry):
+        def visit(i, c):
+            @pl.when(i * n_chunks + n >= used)
+            def _():
+                use(i * n_chunks + n, 0)
+
+            return c
+
+        lax.fori_loop(0, n_reg, visit, 0)
+        return finish(n, carry)
+
+    lax.fori_loop(0, n_chunks, rest, 0)
 
     def partial(cc, s):
         block = nbuf[:, cc, s].reshape(n_x * rows, heads_here * vdim)
@@ -529,15 +540,16 @@
         out_specs=in_vmem,
         scratch_shapes=[
             pltpu.VMEM((seqs, n_tp, rows, width), bf16),
-            pltpu.VMEM((seqs, n_tp, rows, 3 * heads_here * vdim), bf16),
-            pltpu.VMEM((n_chunks, half, rows, vdim), bf16),
-            pltpu.VMEM((n_sp, n_tp, rows, 2 * vdim), bf16),
+            pltpu.VMEM((n_pairs, 2 * chunk, vdim), bf16),
+            pltpu.VMEM((n_pairs, 2, 2 * chunk, vdim), bf16),
+            pltpu.VMEM((n_chunks, chunk, vdim), bf16),
+            pltpu.VMEM((n_sp, 2, 2 * chunk, vdim), bf16),
             pltpu.VMEM((n_chunks, n_tp // 4, 2, rows, vdim), bf16),
             pltpu.VMEM((n_tp // 2, 2, seqs, rows, heads_here * vdim), bf16),
             pltpu.VMEM((8, vdim), f32),
-            pltpu.VMEM((n_chunks, 2 * chunk, vdim), bf16),
-            pltpu.VMEM((n_chunks, 2 * chunk, vdim), f32),
-            pltpu.VMEM((n_chunks, 2 * chunk, 2 * vdim), f32),
+            pltpu.VMEM((n_chunks, vdim, 2 * chunk), bf16),
+            pltpu.VMEM((n_chunks, 8, 2 * chunk), f32),
+            pltpu.VMEM((n_chunks, vdim + 16, 2 * chunk), f32),
             pltpu.VMEM((seqs, n_tp // 2, rows, width), bf16),
             pltpu.VMEM((seqs, n_tp // 2, rows, width), bf16),
             pltpu.VMEM((seqs, n_tp // 2, rows, width), bf16),

time: 209 us -> 190 us (0.909)
  the two profiles are of different devices: /device:TPU:288 before, /device:TPU:33 now
where the time goes in v3:
time: 190 us; the launch traced here: 187 us
  Pallas kernels  181 us (95%)
  local copies, waits for them, and re-layouts  5.68 us (3%)
    pallas_call x1, Pallas kernels, on_device(): pl.pallas_call(functools.partial(layer_kernel, n_sp), name='layer', out_s...  181 us

profile of v3, /device:TPU:33, one launch (start us, length us, event | category | flops | bytes accessed | tf_op | source)
XLA Modules:
  0.0 186.5 jit_solution(13619024528556943987)
XLA Ops:
  0.0 0.0 copy-start
  0.0 0.7 copy-done
  0.7 0.7 broadcast_in_dim.4.lam_ref
  1.3 2.0 %copy.11 = bf16[64,2,2048]{2,0,1:T(8,128)(2,1)} copy(bf16[64,2,2048]{2,1,0:T(2,128)(2,1)} %param.7) | data formatting | bytes 1048576 | tf_op args[0]
  3.3 180.8 %layer.1 = bf16[2,64,2048]{2,1,0:T(8,128)(2,1)} custom-call(bf16[2,64,2048]{2,1,0:T(8,128)(2,1)} %bitcast.6, bf16[2048,256]{1,0:T(8,128)(2,1)} %wq_ref.1, bf16[2048,256]{1,0:T(8,128)(2,1)} %wk_ref.1, bf16[2048,256]{1,0:T(8,128)(2,1)} %wv_ref.1, bf16[256,2048]{1,0:T(8,128)(2,1)} %wo_ref.1, f32[8,128]{1,0:T(8,128)} %broadcast_in_dim.4.lam_ref, f32[1,128]{1,0:T(1,128)} %bitcast.7), custom_call_target="tpu_custom_call" | custom-call | tf_op jit(solution)/shard_map/layer/pallas_call | solution.py:535
  184.2 2.4 %copy.9 = bf16[64,2,2048]{2,1,0:T(2,128)(2,1)} copy(bf16[64,2,2048]{2,0,1:T(8,128)(2,1)} %bitcast.5) | data formatting | bytes 1048576 | tf_op jit(solution)/shard_map/transpose | solution.py:579
  (1 shorter events, 0.0 us)
Async XLA Ops:
  0.0 0.7 copy-start

commit v4 on v3

--- a/solution.py
+++ b/solution.py
@@ -128,7 +128,7 @@
         own, back, fore, far = tp, tp_of(-1, core), tp_of(1, core), tp_of(2, core)
 
         def send(i, src, dst, sem, tt):
-            return to(src, dst, ag_send.at[8 * s + i], sem, z, tt)
+            return to(src, dst, ag_send.at[10 * s + i], sem, z, tt)
 
         sib = 2 * x + 1 - core
 
@@ -136,33 +136,40 @@
             return send(i, tok.at[s, t], tok.at[s, t], ag_recv.at[groups * s + t], tt)
 
         return (
-            lambda: send(0, turned.at[s], tok.at[s, own], ag_recv.at[groups * s + own], fore),
-            lambda: send(1, turned.at[s], tok.at[s, own], ag_recv.at[groups * s + own], back),
+            lambda: send(0, turned.at[s, low], tok.at[s, own, low], ag_half.at[6 * s + 2], fore),
+            lambda: send(1, turned.at[s, high], tok.at[s, own, high], ag_half.at[6 * s + 4], back),
             lambda: send(2, turned.at[s], tok.at[s, own], ag_recv.at[groups * s + own], sib),
-            lambda: send(3, tok.at[s, back, low], tok.at[s, back, low], ag_half.at[2 * s], fore),
-            lambda: send(4, tok.at[s, fore, high], tok.at[s, fore, high], ag_half.at[2 * s + 1], back),
+            lambda: send(3, tok.at[s, back, low], tok.at[s, back, low], ag_half.at[6 * s], fore),
+            lambda: send(4, tok.at[s, fore, high], tok.at[s, fore, high], ag_half.at[6 * s + 1], back),
             lambda: full(5, back, sib),
             lambda: full(6, fore, sib),
             lambda: full(7, far, sib),
+            lambda: send(8, turned.at[s, high], tok.at[s, own, high], ag_half.at[6 * s + 3], fore),
+            lambda: send(9, turned.at[s, low], tok.at[s, own, low], ag_half.at[6 * s + 5], back),
         )
 
     def gather_start(s):
         pltpu.make_async_copy(turned.at[s], tok.at[s, tp], ag_recv.at[groups * s + tp]).start()
-        for copy in gather_copies(s)[:3]:
-            copy().start()
+        copies = gather_copies(s)
+        for i in (0, 1, 8, 9, 2):
+            copies[i]().start()
 
     def gather_near(s):
         copies = gather_copies(s)
-        for i, ahead in enumerate((-1, 1)):
-            t = tp_of(ahead, core)
-            got(tok.at[s, t], ag_recv.at[groups * s + t])
-            copies[3 + i]().start()
-            copies[5 + i]().start()
+        back, fore = tp_of(-1, core), tp_of(1, core)
+        got(tok.at[s, back, low], ag_half.at[6 * s + 2])
+        copies[3]().start()
+        got(tok.at[s, fore, high], ag_half.at[6 * s + 4])
+        copies[4]().start()
+        got(tok.at[s, back, high], ag_half.at[6 * s + 3])
+        copies[5]().start()
+        got(tok.at[s, fore, low], ag_half.at[6 * s + 5])
+        copies[6]().start()
 
     def gather_far(s):
         t = tp_of(2, core)
-        got(tok.at[s, t, low], ag_half.at[2 * s])
-        got(tok.at[s, t, high], ag_half.at[2 * s + 1])
+        got(tok.at[s, t, low], ag_half.at[6 * s])
+        got(tok.at[s, t, high], ag_half.at[6 * s + 1])
         gather_copies(s)[7]().start()
         got(tok.at[s, tp], ag_recv.at[groups * s + tp])
         for ahead in (0, 1, -1, 2):
@@ -556,8 +563,8 @@
             pltpu.VMEM((6 * seqs, rows // 2, width), bf16),
             pltpu.VMEM((6 * seqs, rows // 2, width), bf16),
             dma((seqs * n_tp,)),
-            dma((2 * seqs,)),
-            dma((8 * seqs,)),
+            dma((6 * seqs,)),
+            dma((10 * seqs,)),
             dma((n_sp,)),
             dma((n_chunks,)),
             dma((2 * n_pairs,)),

time: 190 us -> 188 us (0.989)
  Pallas kernels: 181 us -> 179 us
where the time goes in v4:
time: 188 us; the launch traced here: 185 us
  Pallas kernels  179 us (95%)
  local copies, waits for them, and re-layouts  5.68 us (3%)
    pallas_call x1, Pallas kernels, on_device(): pl.pallas_call(functools.partial(layer_kernel, n_sp), name='layer', out_s...  179 us

profile of v4, /device:TPU:33, one launch (start us, length us, event | category | flops | bytes accessed | tf_op | source)
XLA Modules:
  0.0 184.7 jit_solution(8442134289226423006)
XLA Ops:
  0.0 0.0 copy-start
  0.0 0.7 copy-done
  0.7 0.7 broadcast_in_dim.4.lam_ref
  1.3 2.0 %copy.11 = bf16[64,2,2048]{2,0,1:T(8,128)(2,1)} copy(bf16[64,2,2048]{2,1,0:T(2,128)(2,1)} %param.7) | data formatting | bytes 1048576 | tf_op args[0]
  3.3 179.0 %layer.1 = bf16[2,64,2048]{2,1,0:T(8,128)(2,1)} custom-call(bf16[2,64,2048]{2,1,0:T(8,128)(2,1)} %bitcast.6, bf16[2048,256]{1,0:T(8,128)(2,1)} %wq_ref.1, bf16[2048,256]{1,0:T(8,128)(2,1)} %wk_ref.1, bf16[2048,256]{1,0:T(8,128)(2,1)} %wv_ref.1, bf16[256,2048]{1,0:T(8,128)(2,1)} %wo_ref.1, f32[8,128]{1,0:T(8,128)} %broadcast_in_dim.4.lam_ref, f32[1,128]{1,0:T(1,128)} %bitcast.7), custom_call_target="tpu_custom_call" | custom-call | tf_op jit(solution)/shard_map/layer/pallas_call | solution.py:542
  182.3 2.4 %copy.9 = bf16[64,2,2048]{2,1,0:T(2,128)(2,1)} copy(bf16[64,2,2048]{2,0,1:T(8,128)(2,1)} %bitcast.5) | data formatting | bytes 1048576 | tf_op jit(solution)/shard_map/transpose | solution.py:586
  (1 shorter events, 0.0 us)
Async XLA Ops:
  0.0 0.7 copy-start
